TPU v7x, 32 devices: a whole 2x2x4 slice. The times are simulated.
32 devices in a mesh: ep: 8 (over z, x), tp: 4 (over y, core).
Axes of the slice: x: 2, y: 2, z: 4, core: 2. Of those that a mesh axis runs over, the one named last changes fastest.
Arguments:
- mixer_in: bfloat16 [1024, 2048], P('ep'), may hold values from -6 to 6
- mixer_gain: float32 [2048], replicated, may hold values from 0.1 to 1.9
- w_value: bfloat16 [2048, 1536], P(None, 'tp'), may hold values from -0.125 to 0.125
- w_gate: bfloat16 [2048, 1536], P(None, 'tp'), may hold values from -0.125 to 0.125
- w_taps: float32 [31, 1536], P(None, 'tp'), may hold values from -3 to 3
- channel_gain: float32 [1536], P('tp'), may hold values from 0.1 to 1.9
- w_output: bfloat16 [1536, 2048], P('tp'), may hold values from -0.15625 to 0.15625
- expert_in: bfloat16 [1024, 2048], P('ep'), may hold values from -6 to 6
- expert_gain: float32 [2048], replicated, may hold values from 0 to 8
- route_experts: int32 [1024, 4], P('ep'), may hold values from 0 to 7, all different within a row; in each aligned block of 128 rows (0 to 127, 128 to 255, ...) at most 128 rows name the same one
- route_scores: float32 [1024, 4], P('ep'), may hold values from -6 to 6
- expert_gate: bfloat16 [8, 2048, 2048], P('ep', None, 'tp'), may hold values from -0.125 to 0.125
- expert_up: bfloat16 [8, 2048, 2048], P('ep', None, 'tp'), may hold values from -0.125 to 0.125
- expert_down: bfloat16 [8, 2048, 2048], P('ep', 'tp'), may hold values from -0.125 to 0.125
Outputs:
- mixer_out: bfloat16 [1024, 2048], P('ep')
- expert_out: bfloat16 [1024, 2048], P('ep')
Inputs may be any that keep to these rules, and one draw needn't show every extreme that they name: `route_experts`: each row names 4 different experts. In each aligned block of 128 rows (the rows of one index of ep) no expert is named more than 128 times, a bound that some block reaches.
All inputs are finite; a program needn't handle non-finite values.
Results may differ from a plain program's by a relative error of at most 0.02.
Values may be sent and summed in bfloat16 or wider, within the bound.
A program may use at most 64 MiB of HBM per device.

v0:
```python
import jax
import jax.numpy as jnp
from jax import lax
from jax.sharding import PartitionSpec as P

CONV_CH = 1536
CONV_W = 31
TOP_K = 4


epsilon = 1e-05
clamp_limit = 7.0
swish_slope = 1.702


def shifted(block, axis, distance):
    devices = range(lax.axis_size(axis))
    route = [(i - distance, i) for i in devices if i - distance in devices]
    return lax.ppermute(block, axis, route)


def row_norm(inputs, gains):
    widened = inputs.astype(jnp.float32)
    row_mean = jnp.mean(widened, axis=-1, keepdims=True)
    row_var = jnp.mean(jnp.square(widened - row_mean), axis=-1, keepdims=True)
    return (widened - row_mean) * lax.rsqrt(row_var + epsilon) * gains


def local(
    mixer_in,
    mixer_gain,
    w_value,
    w_gate,
    w_taps,
    channel_gain,
    w_output,
    expert_in,
    expert_gain,
    route_experts,
    route_scores,
    expert_gate,
    expert_up,
    expert_down,
):
    normed = row_norm(mixer_in, mixer_gain).astype(jnp.bfloat16)
    values = jnp.dot(normed, w_value, preferred_element_type=jnp.float32)
    gate_pre = jnp.dot(normed, w_gate, preferred_element_type=jnp.float32)
    gated_values = (values * jax.nn.sigmoid(gate_pre)).astype(jnp.bfloat16)
    mixer_rows = gated_values.shape[0]
    reach_rows = CONV_W - 1
    earlier = shifted(gated_values[mixer_rows - reach_rows :], "ep", 1)
    extended = jnp.concatenate([earlier, gated_values], axis=0)
    conv_out = jnp.zeros(gated_values.shape, jnp.float32)
    for offset in range(CONV_W):
        conv_out = (
            conv_out + extended[offset : offset + mixer_rows].astype(jnp.float32) * w_taps[offset]
        )
    channel_sums = lax.psum(
        (
            jnp.sum(conv_out, axis=1, keepdims=True),
            jnp.sum(conv_out * conv_out, axis=1, keepdims=True),
        ),
        "tp",
    )
    row_mean = channel_sums[0] / CONV_CH
    row_var = channel_sums[1] / CONV_CH - row_mean * row_mean
    activated = jax.nn.silu(
        (conv_out - row_mean) * lax.rsqrt(row_var + epsilon) * channel_gain
    ).astype(jnp.bfloat16)
    mixer_out = lax.psum(
        jnp.dot(activated, w_output, preferred_element_type=jnp.float32).astype(jnp.bfloat16), "tp"
    )
    rows_b = expert_in.shape[0]
    width = expert_in.shape[1]
    experts = lax.axis_size("ep")
    capacity = 2 * rows_b * TOP_K // experts
    slot_share = capacity // lax.axis_size("tp")
    column = lax.axis_index("tp")
    normed_b = row_norm(expert_in, expert_gain).astype(jnp.bfloat16)
    raised = jnp.exp(route_scores)
    route_weights = raised / jnp.sum(raised, axis=1, keepdims=True)
    flat_ids = route_experts.reshape(-1)
    onehot = (flat_ids[:, None] == jnp.arange(experts, dtype=jnp.int32)[None, :]).astype(jnp.int32)
    slot_index = jnp.sum((jnp.cumsum(onehot, axis=0) - onehot) * onehot, axis=1)
    owner_row = jnp.arange(rows_b * TOP_K, dtype=jnp.int32) // TOP_K
    slot_table = (
        jnp.full((capacity * experts,), rows_b, jnp.int32)
        .at[slot_index * experts + flat_ids]
        .set(owner_row)
    )
    padded = jnp.concatenate([normed_b, jnp.zeros((1, width), jnp.bfloat16)], axis=0)
    gate_w = expert_gate[0]
    up_w = expert_up[0]
    down_w = expert_down[0]
    own_table = lax.dynamic_slice_in_dim(
        slot_table, column * slot_share * experts, slot_share * experts
    )
    sending = jnp.take(padded, own_table, axis=0).reshape(slot_share, experts, width)
    arrived = lax.all_to_all(sending, "ep", split_axis=1, concat_axis=1, tiled=True)
    block_rows = lax.all_gather(arrived, "tp", axis=0, tiled=True)
    flat_rows = block_rows.reshape(block_rows.shape[0] * block_rows.shape[1], block_rows.shape[2])
    gate_e = jnp.minimum(
        jnp.dot(flat_rows, gate_w, preferred_element_type=jnp.float32), clamp_limit
    )
    up_e = jnp.clip(
        jnp.dot(flat_rows, up_w, preferred_element_type=jnp.float32), -clamp_limit, clamp_limit
    )
    hidden = (
        ((up_e + 1.0) * gate_e * jax.nn.sigmoid(swish_slope * gate_e))
        .astype(jnp.bfloat16)
        .reshape(block_rows.shape[0], block_rows.shape[1], gate_w.shape[1])
        .reshape(capacity * experts, gate_w.shape[1])
    )
    summed = lax.psum_scatter(
        jnp.dot(hidden, down_w, preferred_element_type=jnp.float32).astype(jnp.bfloat16),
        "tp",
        scatter_dimension=0,
        tiled=True,
    )
    returned = lax.all_to_all(
        summed.reshape(slot_share, experts, width), "ep", split_axis=1, concat_axis=1, tiled=True
    )
    every_slot = lax.all_gather(returned, "tp", axis=0, tiled=True).reshape(
        capacity * experts, width
    )
    picked = jnp.take(every_slot, slot_index * experts + flat_ids, axis=0)
    picked = picked.reshape(rows_b, TOP_K, width).astype(jnp.float32)
    expert_out = jnp.sum(picked * route_weights[:, :, None], axis=1).astype(jnp.bfloat16)
    return (mixer_out, expert_out)


def solution(mesh):
    in_specs = (
        P("ep", None),
        P(),
        P(None, "tp"),
        P(None, "tp"),
        P(None, "tp"),
        P("tp"),
        P("tp", None),
        P("ep", None),
        P(),
        P("ep", None),
        P("ep", None),
        P("ep", None, "tp"),
        P("ep", None, "tp"),
        P("ep", "tp", None),
    )
    out_specs = (P("ep", None), P("ep", None))
    return jax.shard_map(local, mesh=mesh, in_specs=in_specs, out_specs=out_specs, check_vma=False)
```

profile of v0, /device:TPU:0, one launch (start us, length us, event | category | flops | bytes accessed | tf_op | source)
XLA Modules:
  0.0 263.1 jit_solution(18099323295168561547)
XLA Ops:
  7.2 0.0 copy-start
  7.2 0.0 all-gather.3.cloned.1.call-start
  7.2 0.9 copy.33
  8.2 0.1 eq.29
  8.3 0.1 eq.25
  8.4 0.1 reshape.119
  8.5 1.1 reduce-window.6
  9.7 0.2 slice_reduce_fusion
  9.9 0.1 fusion.68
  10.0 2.4 scatter_custom_fusion
  12.5 0.1 compare_and_fusion
  12.6 1.2 convert_reduce_fusion
  13.8 1.3 fusion.24
  15.1 0.1 broadcast_in_dim.49
  15.2 0.1 copy.38
  15.3 1.4 fusion.26
  16.8 2.3 gather_fusion
  19.1 2.4 copy_select_fusion
  21.6 32.8 %all_to_all.10 = bf16[32,8,2048]{2,0,1:T(8,128)(2,1)S(1)} all-to-all(bf16[32,8,2048]{2,0,1:T(8,128)(2,1)S(1)} %copy_select_fusion), channel_id=1, replica_groups=mesh['ep'=8,'tp'=4] {'ep'}, dimensions={1} | all-to-all | bytes 2097152 | tf_op jit(solution)/shard_map/all_to_all | solution.py:99
  54.4 1.6 copy.40
  56.0 0.0 all-gather.3.cloned.1.call-update
  56.0 0.0 reduce-scatter.2.cloned.1.call-start
  56.0 33.6 %all-gather.3.cloned.1.call-done = bf16[128,8,2048]{2,1,0:T(8,128)(2,1)} async-done(((bf16[32,8,2048]{2,1,0:T(8,128)(2,1)}), bf16[128,8,2048]{2,1,0:T(8,128)(2,1)}) %all-gather.3.cloned.1.call-update) | async-done | bytes 4194320 | tf_op jit(solution)/shard_map/all_gather | solution.py:100
  89.7 6.6 %fusion.2 = f32[1024,512]{1,0:T(8,128)} fusion(bf16[128,8,2048]{2,1,0:T(8,128)(2,1)} %all-gather.3.cloned.1.call-done, bf16[1,2048,512]{2,1,0:T(8,128)(2,1)} %param.26), kind=kOutput, calls=%fused_computation.5 | convolution fusion | flops 2147483648 | bytes 8388608 | tf_op jit(solution)/shard_map/dot_general | solution.py:106
  96.2 0.0 copy-done
  96.2 10.3 %convolution_convert_fusion = bf16[1024,2048]{1,0:T(8,128)(2,1)} fusion(bf16[1,512,2048]{2,1,0:T(8,128)(2,1)S(1)} %copy-done, f32[1024,512]{1,0:T(8,128)} %fusion.2, bf16[1,2048,512]{2,1,0:T(8,128)(2,1)} %param.25, bf16[128,8,2048]{2,1,0:T(8,128)(2,1)} %all-gather.3.cloned.1.call-done), kind=kOutput, calls=%fused_computation.8 | convolution fusion | flops 4302307328 | bytes 14680064 | tf_op jit(solution)/shard_map/dot_general | solution.py:115
  106.5 0.0 reduce-scatter.2.cloned.1.call-update
  106.6 0.0 all-gather.5.cloned.1.call-start
  106.6 44.7 %reduce-scatter.2.cloned.1.call-done = bf16[256,2048]{1,0:T(8,128)(2,1)} async-done(((bf16[1024,2048]{1,0:T(8,128)(2,1)}), bf16[256,2048]{1,0:T(8,128)(2,1)}) %reduce-scatter.2.cloned.1.call-update) | async-done | bytes 1048592 | tf_op jit(solution)/shard_map/reduce_scatter | solution.py:114
  151.3 1.8 copy.41
  153.1 30.9 %all_to_all.11 = bf16[32,8,2048]{2,0,1:T(8,128)(2,1)S(1)} all-to-all(bf16[32,8,2048]{2,0,1:T(8,128)(2,1)S(1)} %copy.41), channel_id=1, replica_groups=mesh['ep'=8,'tp'=4] {'ep'}, dimensions={1} | all-to-all | bytes 2097152 | tf_op jit(solution)/shard_map/all_to_all | solution.py:120
  184.0 1.6 copy.42
  185.6 0.0 all-gather.5.cloned.1.call-update
  185.6 0.2 all-reduce.4.cloned.1.call-start
  185.8 0.0 copy-done.1
  185.9 0.0 copy-start.5
  185.9 0.2 convert_reduce_fusion.1
  186.0 0.3 fusion.27
  186.3 0.0 copy-done.6
  186.3 1.9 fusion.81
  188.2 0.0 copy-done.5
  188.3 0.0 copy-start.4
  188.3 0.0 copy-start.2
  188.3 0.0 copy-start.3
  188.3 0.0 copy-start.7
  188.3 0.5 fusion.23
  188.9 3.4 %collective-permute-start = (bf16[30,384]{1,0:T(8,128)(2,1)S(1)}, bf16[30,384]{1,0:T(8,128)(2,1)S(1)}, u32[]{:S(2)}, u32[]{:S(2)}) collective-permute-start(bf16[30,384]{1,0:T(8,128)(2,1)S(1)} %slice.260), channel_id=1, source_target_pairs={{0,4},{4,8},{8,12},{12,16},{16,20},{20,24},{24,28},{1,5},{5,9},{9,... | collective-permute-start | bytes 69128 | tf_op jit(solution)/shard_map/ppermute | solution.py:19
  192.2 0.1 mul.528
  192.4 0.1 copy.35
  192.5 0.1 slice_reduce_fusion.30
  192.5 0.1 slice_reduce_fusion.31
  192.7 0.1 copy.36
  192.8 0.1 copy.43
  192.9 0.8 collective-permute-done
  193.7 0.9 fusion.83
  194.7 6.5 %all-reduce.1 = (f32[128,1]{0,1:T(1,128)S(1)}, f32[128,1]{0,1:T(1,128)S(1)}) all-reduce(f32[128,1]{0,1:T(1,128)S(1)} %bitcast.51, f32[128,1]{0,1:T(1,128)S(1)} %bitcast.50), channel_id=1, replica_groups=mesh['ep'=8,'tp'=4] {'tp'}, use_global_device_ids=true, to_apply=%region_5.0 | all-reduce | flops 256 | bytes 2048 | tf_op jit(solution)/shard_map/psum | solution.py:58
  201.1 2.7 %convolution_convert_fusion.1 = bf16[128,2048]{1,0:T(8,128)(2,1)} fusion(bf16[384,2048]{1,0:T(8,128)(2,1)} %param.20, f32[128,384]{1,0:T(8,128)S(1)} %get-tuple-element.39, f32[384]{0:T(512)S(1)} %copy-done.7, f32[128]{0:T(128)S(1)} %get-tuple-element.41, f32[128]{0:T(128)S(1)} %get-tuple-element.40), kind=kOutput, calls=%fused_computation.9 | convolution fusion | flops 201981952 | bytes 2296320 | tf_op jit(solution)/shard_map/dot_general | solution.py:71
  203.9 0.0 all-reduce.4.cloned.1.call-update
  203.9 14.5 %all-gather.5.cloned.1.call-done = bf16[128,8,2048]{2,1,0:T(8,128)(2,1)} async-done(((bf16[32,8,2048]{2,1,0:T(8,128)(2,1)}), bf16[128,8,2048]{2,1,0:T(8,128)(2,1)}) %all-gather.5.cloned.1.call-update) | async-done | bytes 4194320 | tf_op jit(solution)/shard_map/all_gather | solution.py:123
  218.4 8.0 %gather_fusion.1 = bf16[512,2048]{1,0:T(8,128)(2,1)} fusion(bf16[1024,2048]{1,0:T(8,128)(2,1)} %bitcast.44, s32[1024]{0:T(1024)S(1)} %pad_clamp_fusion), kind=kCustom, calls=%fused_computation.1 | custom fusion | bytes 4196352 | tf_op jit(solution)/shard_map/jit(_take)/gather | solution.py:126
  226.4 4.1 %gather.15 = bf16[128,4,2048]{2,1,0:T(4,128)(2,1)} reshape(bf16[512,2048]{1,0:T(8,128)(2,1)} %gather_fusion.1) | data formatting | bytes 4194304 | tf_op jit(solution)/shard_map/jit(_take)/gather | solution.py:126
  230.6 6.4 %multiply_reduce_fusion = bf16[128,2048]{1,0:T(8,128)(2,1)} fusion(f32[128,4]{1,0:T(8,128)S(1)} %copy.43, bf16[128,4,2048]{2,1,0:T(4,128)(2,1)} %gather.15, pred[128,4]{1,0:T(8,128)(4,1)S(1)} %copy.36), kind=kLoop, calls=%fused_computation.7 | loop fusion | flops 3932160 | bytes 2624000 | tf_op jit(solution)/shard_map/reduce_sum | solution.py:128
  237.0 17.7 %all-reduce.4.cloned.1.call-done = bf16[128,2048]{1,0:T(8,128)(2,1)} async-done(((bf16[128,2048]{1,0:T(8,128)(2,1)}), bf16[128,2048]{1,0:T(8,128)(2,1)}) %all-reduce.4.cloned.1.call-update) | async-done | bytes 524304 | tf_op jit(solution)/shard_map/psum | solution.py:70
  254.7 1.9 copy.46
  (24 shorter events, 0.2 us)
Async XLA Ops:
  7.2 89.1 %copy-start = (bf16[1,512,2048]{2,1,0:T(8,128)(2,1)S(1)}, bf16[1,512,2048]{2,1,0:T(8,128)(2,1)}, u32[]{:S(2)}) copy-start(bf16[1,512,2048]{2,1,0:T(8,128)(2,1)} %param.27) | copy-start | bytes 6291460
  7.2 82.5 %all-gather.3.cloned.1.call-start = ((), (), s32[]{:S(2)}) async-start(), calls=%async_computation.4 | async-start | bytes 5242880 | tf_op jit(solution)/shard_map/all_gather | solution.py:100
  56.0 95.3 %reduce-scatter.2.cloned.1.call-start = ((), (), s32[]{:S(2)}) async-start(), calls=%async_computation.5 | async-start | bytes 5242880 | tf_op jit(solution)/shard_map/reduce_scatter | solution.py:114
  106.6 111.9 %all-gather.5.cloned.1.call-start = ((), (), s32[]{:S(2)}) async-start(), calls=%async_computation.6 | async-start | bytes 5242880 | tf_op jit(solution)/shard_map/all_gather | solution.py:123
  184.0 1.8 copy-start.1
  184.0 2.3 copy-start.6
  185.6 69.1 %all-reduce.4.cloned.1.call-start = ((), (), s32[]{:S(2)}) async-start(), calls=%async_computation.3 | async-start | bytes 1048576 | tf_op jit(solution)/shard_map/psum | solution.py:70
  185.9 2.4 copy-start.5
  188.3 4.2 %copy-start.4 = (f32[128,4]{0,1:T(4,128)S(1)}, f32[128,4]{0,1:T(4,128)}, u32[]{:S(2)}) copy-start(f32[128,4]{0,1:T(4,128)} %param.24) | copy-start | bytes 6148
  188.3 4.2 %copy-start.2 = (f32[31,384]{1,0:T(8,128)S(1)}, f32[31,384]{1,0:T(8,128)}, u32[]{:S(2)}) copy-start(f32[31,384]{1,0:T(8,128)} %param.18) | copy-start | bytes 142852
  188.3 4.4 %copy-start.3 = (s32[128,4]{0,1:T(4,128)S(1)}, s32[128,4]{0,1:T(4,128)}, u32[]{:S(2)}) copy-start(s32[128,4]{0,1:T(4,128)} %param.23) | copy-start | bytes 6148
  188.3 12.9 %copy-start.7 = (f32[384]{0:T(512)S(1)}, f32[384]{0:T(512)}, u32[]{:S(2)}) copy-start(f32[384]{0:T(512)} %param.19) | copy-start | bytes 4612
  188.9 4.9 %collective-permute-start = (bf16[30,384]{1,0:T(8,128)(2,1)S(1)}, bf16[30,384]{1,0:T(8,128)(2,1)S(1)}, u32[]{:S(2)}, u32[]{:S(2)}) collective-permute-start(bf16[30,384]{1,0:T(8,128)(2,1)S(1)} %slice.260), channel_id=1, source_target_pairs={{0,4},{4,8},{8,12},{12,16},{16,20},{20,24},{24,28},{1,5},{5,9},{9,... | collective-permute-start | bytes 69128 | tf_op jit(solution)/shard_map/ppermute | solution.py:19
Sparse Core Ops, SparseCore 0:
  56.1 33.4 all-gather.2
  106.7 44.5 reduce-scatter.1
  185.7 32.6 all-gather.4
  221.2 33.4 all-reduce.3
where the time goes:
time: 264 us; the launch traced here: 263 us
  waiting for transfers between devices  111 us (42%)
  blocking collectives  70.2 us (27%)
  local copies, waits for them, and re-layouts  26 us (10%)
  matrix products  22.1 us (8%)
  other arithmetic  15.7 us (6%)
  between operations  14 us (5%)
  starting transfers between devices  3.71 us (1%)
    reduce_scatter x1, waiting for transfers between devices, local(): lax.psum_scatter(jnp.dot(hidden, down_w, preferred_element_type=jnp.float...  44.7 us
    all_gather x1, waiting for transfers between devices, local(): block_rows = lax.all_gather(arrived, 'tp', axis=0, tiled=True)  33.6 us
    all_to_all x1, blocking collectives, local(): lax.all_to_all(sending, 'ep', split_axis=1, concat_axis=1, tiled=True)  32.8 us
    all_to_all x1, blocking collectives, local(): lax.all_to_all(summed.reshape(slot_share, experts, width), 'ep', split_ax...  30.9 us
    psum x1, waiting for transfers between devices, local(): lax.psum(jnp.dot(activated, w_output, preferred_element_type=jnp.float32)...  17.7 us
    all_gather x1, waiting for transfers between devices, local(): lax.all_gather(returned, 'tp', axis=0, tiled=True)  14.5 us
    gather x2, local copies, waits for them, and re-layouts, local(): picked = jnp.take(every_slot, slot_index * experts + flat_ids, axis=0)  12.1 us
    dot_general x1, matrix products, local(): jnp.dot(hidden, down_w, preferred_element_type=jnp.float32)  10.3 us
  transfers between devices with their start and end apart: 5, of which 5 were waited for; matrix products, arithmetic and copies ran while one was open for 10% of the time, Pallas kernels for 0%

commit v1 on v0

--- a/solution.py
+++ b/solution.py
@@ -1,6 +1,10 @@
+import functools
+
 import jax
 import jax.numpy as jnp
 from jax import lax
+from jax.experimental import pallas as pl
+from jax.experimental.pallas import tpu as pltpu
 from jax.sharding import PartitionSpec as P
 
 CONV_CH = 1536
@@ -129,7 +133,438 @@
     return (mixer_out, expert_out)
 
 
+MESH = pl.DeviceIdType.MESH
+QUARTERS = 4
+HALO = 32
+
+
+def kernel(
+    ep,
+    tp,
+    mixer_in,
+    mixer_gain,
+    w_value,
+    w_gate,
+    w_taps,
+    channel_gain,
+    w_output,
+    expert_in,
+    expert_gain,
+    route_experts,
+    route_scores,
+    expert_gate,
+    expert_up,
+    expert_down,
+    mixer_out,
+    expert_out,
+    wv,
+    wg,
+    wo,
+    eg,
+    eu,
+    ed,
+    load_sem,
+    send_sem,
+    recv_sem,
+    tokens,
+    shares,
+    gated_tail,
+    halo,
+    extended,
+    conv,
+    stats,
+    mixer_part,
+    mixer_core,
+    mixer_y,
+    mixer_all,
+    hidden,
+    parts,
+    part_core,
+    part_y,
+    part_x,
+    part_ring,
+    expert_y,
+    expert_all,
+):
+    rows = mixer_in.shape[0]
+    width = mixer_in.shape[1] // QUARTERS
+    depth = ep // 2
+    me = lax.axis_index("ep")
+    col = lax.axis_index("tp")
+    z, x = lax.div(me, 2), lax.rem(me, 2)
+    y, core = lax.div(col, 2), lax.rem(col, 2)
+    z_next = (lax.rem(z + 1, depth) * 2 + x, col)
+    x_peer = (z * 2 + 1 - x, col)
+    y_peer = (me, (1 - y) * 2 + core)
+    core_peer = (me, y * 2 + 1 - core)
+    own_q, other_q = 2 * core + y, 2 * core + 1 - y
+    own_half, other_half = pl.ds(2 * core, 2), pl.ds(2 * (1 - core), 2)
+    f32, bf16 = jnp.float32, jnp.bfloat16
+
+    def behind(steps):
+        return lax.rem(z + depth - steps, depth)
+
+    sent = []
+
+    def send(src, dst, device):
+        i = len(sent)
+        copy = pltpu.make_async_remote_copy(
+            src_ref=src,
+            dst_ref=dst,
+            send_sem=send_sem.at[i],
+            recv_sem=recv_sem.at[i],
+            device_id=device,
+            device_id_type=MESH,
+        )
+        copy.start()
+        sent.append(copy)
+        return copy
+
+    barrier = pltpu.get_barrier_semaphore()
+    for d in range(1, ep):
+        pl.semaphore_signal(
+            barrier, inc=1, device_id=(lax.rem(me + d, ep), col), device_id_type=MESH
+        )
+    for d in range(1, tp):
+        pl.semaphore_signal(
+            barrier, inc=1, device_id=(me, lax.rem(col + d, tp)), device_id_type=MESH
+        )
+
+    loads = [
+        pltpu.make_async_copy(src, dst, load_sem.at[i])
+        for i, (src, dst) in enumerate(
+            (
+                (w_value, wv),
+                (w_gate, wg),
+                (w_output, wo),
+                (expert_gate.at[0], eg),
+                (expert_up.at[0], eu),
+                (expert_down.at[0], ed),
+            )
+        )
+    ]
+    for load in loads:
+        load.start()
+
+    def norm(ref, gain):
+        widened = ref[...].astype(f32)
+        mean = jnp.mean(widened, axis=-1, keepdims=True)
+        centred = widened - mean
+        var = jnp.mean(centred * centred, axis=-1, keepdims=True)
+        return (centred * lax.rsqrt(var + epsilon) * gain[...]).astype(bf16)
+
+    normed = norm(expert_in, expert_gain)
+    for q in range(QUARTERS):
+        tokens[me, q] = normed[:, q * width : (q + 1) * width]
+    raised = jnp.exp(route_scores[...])
+    weights = raised / jnp.sum(raised, axis=1, keepdims=True)
+    ids = route_experts[...]
+    lane = lax.broadcasted_iota(jnp.int32, (rows, rows), 1)
+    dense = jnp.zeros((rows, rows), f32)
+    for k in range(TOP_K):
+        dense = dense + jnp.where(ids[:, k : k + 1] == lane, weights[:, k : k + 1], 0.0)
+    shares[me] = jnp.transpose(dense)[:ep]
+    pl.semaphore_wait(barrier, ep - 1 + tp - 1)
+
+    z_copies, x_copies, y_copies, cz_copies, cx_copies = [], [], [], [None], []
+
+    def send_z(block):
+        part = tokens.at[block, own_half]
+        z_copies.append(send(part, part, z_next))
+
+    def send_x(block):
+        part = tokens.at[block, own_q]
+        x_copies.append(send(part, part, x_peer))
+
+    def send_core(block, copies):
+        part = tokens.at[block, own_half]
+        copies.append(send(part, part, core_peer))
+
+    send_x(me)
+    send_z(me)
+    share_copies = [
+        send(shares.at[me], shares.at[me], (lax.rem(me + d, ep), col)) for d in range(1, ep)
+    ]
+
+    def arrived_z(step):
+        block = behind(step) * 2 + x
+        z_copies[step - 1].wait_recv()
+        if step < depth - 1:
+            send_z(block)
+        send_x(block)
+        send_core(block, cz_copies)
+
+    def arrived_x(step):
+        x_copies[step].wait_recv()
+        part = tokens.at[behind(step) * 2 + 1 - x, own_q]
+        y_copies.append(send(part, part, y_peer))
+
+    def arrived_y(step):
+        y_copies[step].wait_recv()
+        send_core(behind(step) * 2 + 1 - x, cx_copies)
+
+    def share_column(block):
+        row = shares[block, pl.ds(me, 1), :]
+        return jnp.transpose(jnp.broadcast_to(row, (rows, rows)))[:, :1]
+
+    ret_core = []
+
+    def expert_step(step):
+        if step:
+            cz_copies[step].wait_recv()
+        cx_copies[step].wait_recv()
+        first = behind(step) * 2
+        blocks = pl.ds(first, 2)
+        inputs = jnp.concatenate(
+            [tokens[blocks, q].reshape(2 * rows, width) for q in range(QUARTERS)], axis=1
+        )
+        share = jnp.concatenate([share_column(first), share_column(first + 1)], axis=0)
+        chunk = min(256, eg.shape[1])
+        for n in range(0, eg.shape[1], chunk):
+            gate_e = jnp.minimum(
+                jnp.dot(inputs, eg[:, n : n + chunk], preferred_element_type=f32), clamp_limit
+            )
+            up_e = jnp.clip(
+                jnp.dot(inputs, eu[:, n : n + chunk], preferred_element_type=f32),
+                -clamp_limit,
+                clamp_limit,
+            )
+            act = (up_e + 1.0) * gate_e * jax.nn.sigmoid(swish_slope * gate_e)
+            hidden[:, n : n + chunk] = (act * share).astype(bf16)
+        for q in range(QUARTERS):
+            down = jnp.dot(
+                hidden[...], ed[:, q * width : (q + 1) * width], preferred_element_type=f32
+            )
+            parts[blocks, q] = down.astype(bf16).reshape(2, rows, width)
+        ret_core.append(send(parts.at[blocks, other_half], part_core.at[behind(step)], core_peer))
+
+    ret_y, ret_x, ring = {}, {}, []
+
+    def add_to(block, q, term):
+        parts[block, q] = (parts[block, q].astype(f32) + term.astype(f32)).astype(bf16)
+
+    def return_core(step):
+        zi = behind(step)
+        ret_core[step].wait_recv()
+        for b in range(2):
+            for h in range(2):
+                add_to(2 * zi + b, 2 * core + h, part_core[zi, b, h])
+        ret_y[step] = send(parts.at[2 * zi + 1 - x, other_q], part_y.at[zi], y_peer)
+
+    def return_y(step):
+        zi = behind(step)
+        ret_y[step].wait_recv()
+        add_to(2 * zi + 1 - x, own_q, part_y[zi])
+        ret_x[step] = send(parts.at[2 * zi + 1 - x, own_q], part_x.at[zi], x_peer)
+
+    def return_x(step):
+        zi = behind(step)
+        ret_x[step].wait_recv()
+        add_to(2 * zi + x, own_q, part_x[zi])
+
+    def ring_step(step):
+        block = 2 * behind(step) + x
+        if step > 1:
+            ring[step - 2].wait_recv()
+            for h in range(2):
+                add_to(block, 2 * core + h, part_ring[step - 2, h])
+        ring.append(send(parts.at[block, own_half], part_ring.at[step - 1], z_next))
+
+    loads[0].wait()
+    loads[1].wait()
+    normed_a = norm(mixer_in, mixer_gain)
+    values = jnp.dot(normed_a, wv[...], preferred_element_type=f32)
+    gate_pre = jnp.dot(normed_a, wg[...], preferred_element_type=f32)
+    gated = (values * jax.nn.sigmoid(gate_pre)).astype(bf16)
+    gated_tail[...] = gated[rows - HALO :]
+    extended[pl.ds(HALO, rows), :] = gated.astype(f32)
+    halo_copy = send(gated_tail, halo, (lax.rem(me + 1, ep), col))
+
+    arrived_x(0)
+
+    halo_copy.wait_recv()
+    keep = jnp.where(me > 0, 1.0, 0.0).astype(f32)
+    extended[pl.ds(0, HALO), :] = halo[...].astype(f32) * keep
+    channels = w_taps.shape[1]
+    sums = jnp.zeros((rows, 1), f32)
+    squares = jnp.zeros((rows, 1), f32)
+    first = HALO - (CONV_W - 1)
+    for c in range(0, channels, 128):
+        total = jnp.zeros((rows, 128), f32)
+        for offset in range(CONV_W):
+            total = (
+                total
+                + extended[pl.ds(first + offset, rows), c : c + 128]
+                * w_taps[offset : offset + 1, c : c + 128]
+            )
+        conv[:, c : c + 128] = total
+        sums = sums + jnp.sum(total, axis=1, keepdims=True)
+        squares = squares + jnp.sum(total * total, axis=1, keepdims=True)
+    stats[0] = jnp.transpose(jnp.where(lane == 0, sums, jnp.where(lane == 1, squares, 0.0)))[:8]
+    stat_copies = [
+        send(stats.at[0], stats.at[d], (me, lax.rem(col + d, tp))) for d in range(1, tp)
+    ]
+
+    arrived_z(1)
+    arrived_y(0)
+
+    for copy in stat_copies:
+        copy.wait_recv()
+    stat = stats[0]
+    for d in range(1, tp):
+        stat = stat + stats[d]
+    stat = jnp.transpose(jnp.concatenate([stat] * (rows // 8), axis=0))
+    row_mean = stat[:, 0:1] / CONV_CH
+    row_var = stat[:, 1:2] / CONV_CH - row_mean * row_mean
+    activated = jax.nn.silu(
+        (conv[...] - row_mean) * lax.rsqrt(row_var + epsilon) * channel_gain[...]
+    ).astype(bf16)
+    loads[2].wait()
+    for q in range(QUARTERS):
+        mixer_part[q] = jnp.dot(
+            activated, wo[:, q * width : (q + 1) * width], preferred_element_type=f32
+        ).astype(bf16)
+    m_core = send(mixer_part.at[other_half], mixer_core, core_peer)
+
+    for copy in share_copies:
+        copy.wait_recv()
+    for load in loads[3:]:
+        load.wait()
+    expert_step(0)
+
+    def mixer_sum():
+        m_core.wait_recv()
+        for h in range(2):
+            q = 2 * core + h
+            mixer_part[q] = (mixer_part[q].astype(f32) + mixer_core[h].astype(f32)).astype(bf16)
+        return send(mixer_part.at[other_q], mixer_y, y_peer)
+
+    def spread_y(whole):
+        return send(whole.at[own_q], whole.at[own_q], y_peer)
+
+    def spread_core(whole):
+        return send(whole.at[own_half], whole.at[own_half], core_peer)
+
+    arrived_x(1)
+    m_y = mixer_sum()
+    for step in range(1, depth):
+        if step < depth - 1:
+            arrived_z(step + 1)
+        arrived_y(step)
+        return_core(step - 1)
+        if step >= 2:
+            return_y(step - 2)
+        expert_step(step)
+        if step < depth - 1:
+            arrived_x(step + 1)
+        if step == 1:
+            m_y.wait_recv()
+            mixer_all[own_q] = (mixer_part[own_q].astype(f32) + mixer_y[...].astype(f32)).astype(
+                bf16
+            )
+            m_spread = spread_y(mixer_all)
+        if step == 2:
+            m_spread.wait_recv()
+            m_last = spread_core(mixer_all)
+        if step >= 3:
+            return_x(step - 2)
+            ring_step(step - 2)
+
+    last = depth - 1
+    return_y(last - 1)
+    return_core(last)
+    return_x(last - 1)
+    ring_step(last - 1)
+    return_y(last)
+    return_x(0)
+    m_last.wait_recv()
+    for q in range(QUARTERS):
+        mixer_out[:, q * width : (q + 1) * width] = mixer_all[q]
+    return_x(last)
+    ring_step(last)
+    ring[last - 1].wait_recv()
+    for h in range(2):
+        add_to(me, 2 * core + h, part_ring[last - 1, h])
+    e_y = send(parts.at[me, other_q], expert_y, y_peer)
+    e_y.wait_recv()
+    expert_all[own_q] = (parts[me, own_q].astype(f32) + expert_y[...].astype(f32)).astype(bf16)
+    spread_y(expert_all).wait_recv()
+    spread_core(expert_all).wait_recv()
+    for q in range(QUARTERS):
+        expert_out[:, q * width : (q + 1) * width] = expert_all[q]
+    for copy in sent:
+        copy.wait_send()
+
+
+def fused_local(sizes, *args):
+    ep, tp = sizes["ep"], sizes["tp"]
+    mixer_in, w_value, w_taps, w_output = args[0], args[2], args[4], args[6]
+    expert_in, gate_w = args[7], args[11]
+    rows, features = expert_in.shape
+    capacity = 2 * rows * TOP_K // ep
+    if capacity < rows or tp != 4 or ep != 8 or rows != 128:
+        return local(*args)
+    width = features // QUARTERS
+    depth = ep // 2
+    hidden_units = gate_w.shape[2]
+    channels = w_taps.shape[1]
+    f32, bf16 = jnp.float32, jnp.bfloat16
+    vmem = pl.BlockSpec(memory_space=pltpu.VMEM)
+    hbm = pl.BlockSpec(memory_space=pl.ANY)
+    copies = 96
+    tile = (rows, width)
+    args = list(args)
+    for i in (1, 5, 8):
+        args[i] = args[i].reshape(1, -1)
+    flops = 2 * rows * ep * features * hidden_units * 3
+    return pl.pallas_call(
+        functools.partial(kernel, ep, tp),
+        out_shape=(
+            jax.ShapeDtypeStruct(mixer_in.shape, bf16),
+            jax.ShapeDtypeStruct(expert_in.shape, bf16),
+        ),
+        in_specs=[hbm if i in (2, 3, 6, 11, 12, 13) else vmem for i in range(14)],
+        out_specs=(vmem, vmem),
+        scratch_shapes=[
+            pltpu.VMEM(w_value.shape, bf16),
+            pltpu.VMEM(w_value.shape, bf16),
+            pltpu.VMEM(w_output.shape, bf16),
+            pltpu.VMEM((features, hidden_units), bf16),
+            pltpu.VMEM((features, hidden_units), bf16),
+            pltpu.VMEM((hidden_units, features), bf16),
+            pltpu.SemaphoreType.DMA((6,)),
+            pltpu.SemaphoreType.DMA((copies,)),
+            pltpu.SemaphoreType.DMA((copies,)),
+            pltpu.VMEM((ep, QUARTERS) + tile, bf16),
+            pltpu.VMEM((ep, ep, rows), f32),
+            pltpu.VMEM((HALO, channels), bf16),
+            pltpu.VMEM((HALO, channels), bf16),
+            pltpu.VMEM((HALO + rows, channels), f32),
+            pltpu.VMEM((rows, channels), f32),
+            pltpu.VMEM((tp, 8, rows), f32),
+            pltpu.VMEM((QUARTERS,) + tile, bf16),
+            pltpu.VMEM((2,) + tile, bf16),
+            pltpu.VMEM(tile, bf16),
+            pltpu.VMEM((QUARTERS,) + tile, bf16),
+            pltpu.VMEM((2 * rows, hidden_units), bf16),
+            pltpu.VMEM((ep, QUARTERS) + tile, bf16),
+            pltpu.VMEM((depth, 2, 2) + tile, bf16),
+            pltpu.VMEM((depth,) + tile, bf16),
+            pltpu.VMEM((depth,) + tile, bf16),
+            pltpu.VMEM((depth - 1, 2) + tile, bf16),
+            pltpu.VMEM(tile, bf16),
+            pltpu.VMEM((QUARTERS,) + tile, bf16),
+        ],
+        compiler_params=pltpu.CompilerParams(
+            collective_id=0, has_side_effects=True, vmem_limit_bytes=56 * 1024 * 1024
+        ),
+        cost_estimate=pl.CostEstimate(flops=flops, bytes_accessed=1 << 24, transcendentals=0),
+        name="mixer_and_experts",
+    )(*args)
+
+
 def solution(mesh):
+    body = functools.partial(fused_local, dict(mesh.shape))
     in_specs = (
         P("ep", None),
         P(),
@@ -147,4 +582,4 @@
         P("ep", "tp", None),
     )
     out_specs = (P("ep", None), P("ep", None))
-    return jax.shard_map(local, mesh=mesh, in_specs=in_specs, out_specs=out_specs, check_vma=False)
+    return jax.shard_map(body, mesh=mesh, in_specs=in_specs, out_specs=out_specs, check_vma=False)

time: 264 us -> 90 us (0.34)
  waiting for transfers between devices: 111 us -> 0 us
  Pallas kernels: 0 us -> 80.4 us
  blocking collectives: 70.2 us -> 0 us
  matrix products: 22.1 us -> 0 us
  local copies, waits for them, and re-layouts: 26 us -> 7.87 us
  other arithmetic: 15.7 us -> 0 us
  between operations: 14 us -> 0.64 us
  starting transfers between devices: 3.71 us -> 0 us
    pallas_call x0 -> x1, Pallas kernels: none -> 80.4 us  [fused_local(): pl.pallas_call(functools.partial(kernel, ep, tp), out_shape=(jax.ShapeDty...]
    all_to_all x2 -> x0, blocking collectives: 63.8 us -> none  [the longest x1 32.8 us: local(): lax.all_to_all(sending, 'ep', split_axis=1, concat_axis=1, tiled=True)]
    all_gather x2 -> x0, waiting for transfers between devices: 48.1 us -> none  [the longest x1 33.6 us: local(): block_rows = lax.all_gather(arrived, 'tp', axis=0, tiled=True)]
    reduce_scatter x1 -> x0, waiting for transfers between devices: 44.7 us -> none  [local(): lax.psum_scatter(jnp.dot(hidden, down_w, preferred_element_type=jnp.float...]
    dot_general x5 -> x0, matrix products: 22.1 us -> none  [the longest x1 10.3 us: local(): jnp.dot(hidden, down_w, preferred_element_type=jnp.float32)]
    psum x1 -> x0, waiting for transfers between devices: 17.7 us -> none  [local(): lax.psum(jnp.dot(activated, w_output, preferred_element_type=jnp.float32)...]
    gather x3 -> x0, local copies, waits for them, and re-layouts: 14.5 us -> none  [the longest x2 12.1 us: local(): picked = jnp.take(every_slot, slot_index * experts + flat_ids, axis=0)]
    reduce_sum x8 -> x0, other arithmetic: 10.4 us -> none  [the longest x1 6.43 us: local(): jnp.sum(picked * route_weights[:, :, None], axis=1).astype(jnp.bfloat16)]
  transfers between devices with their start and end apart: 5 -> 0, of which waited for: 5 -> 0; matrix products, arithmetic and copies ran while one was open for 10% -> 0% of each run, Pallas kernels for 0% -> 0%
where the time goes in v1:
time: 90 us; the launch traced here: 89 us
  Pallas kernels  80.4 us (89%)
  local copies, waits for them, and re-layouts  7.87 us (9%)
    pallas_call x1, Pallas kernels, fused_local(): pl.pallas_call(functools.partial(kernel, ep, tp), out_shape=(jax.ShapeDty...  80.4 us
    unnamed x4, local copies, waits for them, and re-layouts  6.59 us

profile of v1, /device:TPU:0, one launch (start us, length us, event | category | flops | bytes accessed | tf_op | source)
XLA Modules:
  0.0 89.0 jit_solution(12631369724281117921)
XLA Ops:
  0.6 1.3 %reshape.14.channel_gain = f32[1,384]{1,0:T(1,128)} reshape(f32[384]{0:T(512)} %param.19) | data formatting | bytes 3072 | tf_op jit(solution)/shard_map/reshape | solution.py:518
  1.9 1.4 %copy.16.route_experts = s32[128,4]{1,0:T(8,128)} copy(s32[128,4]{0,1:T(4,128)} %param.23) | data formatting | bytes 4096 | tf_op args[9]
  3.3 1.4 %copy.17.route_scores = f32[128,4]{1,0:T(8,128)} copy(f32[128,4]{0,1:T(4,128)} %param.24) | data formatting | bytes 4096 | tf_op args[10]
  4.7 80.4 %mixer_and_experts.1 = (bf16[128,2048]{1,0:T(8,128)(2,1)}, bf16[128,2048]{1,0:T(8,128)(2,1)}) custom-call(bf16[128,2048]{1,0:T(8,128)(2,1)} %mixer_in.1, f32[1,2048]{1,0:T(1,128)} %bitcast.2, bf16[2048,384]{1,0:T(8,128)(2,1)} %w_value.1, bf16[2048,384]{1,0:T(8,128)(2,1)} %w_gate.1, f32[31,384]{1,0:T(8,128)} %w_taps.1, f32[1,384]{1,0:T(1,128)} %reshape.14.channel_gain, ...), custom_call_target="tpu_custom_call" | custom-call | flops 6442450944 | bytes 16777216 | tf_op jit(solution)/shard_map/mixer_and_experts/pallas_call | solution.py:520
  85.2 1.9 %copy.20 = bf16[128,2048]{1,0:T(8,128)(2,1)} copy(bf16[128,2048]{1,0:T(8,128)(2,1)} %get-tuple-element.4) | data formatting | bytes 1048576
  87.1 1.9 %copy.21 = bf16[128,2048]{1,0:T(8,128)(2,1)} copy(bf16[128,2048]{1,0:T(8,128)(2,1)} %get-tuple-element.5) | data formatting | bytes 1048576
